TPU v7x, 32 devices: a whole 2x2x4 slice. The times are simulated.
32 devices in a mesh: sp: 8 (over z, x), tp: 4 (over y, core).
Axes of the slice: x: 2, y: 2, z: 4, core: 2. Of those that a mesh axis runs over, the one named last changes fastest.
Arguments:
- tokens: bfloat16 [2048, 2048], P('sp', 'tp'), may hold values from -6 to 6
- norm_gain: float32 [2048], replicated, may hold values from 0.1 to 1.9
- query_one: bfloat16 [2048, 512], P('sp', 'tp'), may hold values from -1 to 1
- key_one: bfloat16 [2048, 512], P('sp', 'tp'), may hold values from -1 to 1
- query_two: bfloat16 [2048, 512], P('sp', 'tp'), may hold values from -0.15625 to 0.15625
- key_two: bfloat16 [2048, 512], P('sp', 'tp'), may hold values from -0.15625 to 0.15625
- value_weight: bfloat16 [2048, 1024], P('sp', 'tp'), may hold values from -0.5 to 0.5
- pool_weight: bfloat16 [2048, 1024], P('sp', 'tp'), may hold values from -0.125 to 0.125
- lambda_head: float32 [8], replicated, may hold values from 0.3 to 0.8
- head_gain: float32 [128], replicated, may hold values from 0.1 to 1.9
- group_weight: bfloat16 [8, 128, 128], replicated, may hold values from -0.5 to 0.5
- pool_scale: float32 [1024], replicated, may hold values from 0.1 to 1.9
- out_attn: bfloat16 [1024, 2048], P('tp', 'sp'), may hold values from -0.125 to 0.125
- out_pool: bfloat16 [1024, 2048], P('tp', 'sp'), may hold values from -0.125 to 0.125
Outputs:
- mixed: bfloat16 [2048, 2048], P(('sp', 'tp'))
All inputs are finite; a program needn't handle non-finite values.
Results may differ from a plain program's by a relative error of at most 0.013.
Values may be sent and summed in bfloat16 or wider, within the bound.
A program may use at most 128 MiB of HBM per device.

v0:
```python
import math
import jax
import jax.numpy as jnp
from jax import lax
from jax.sharding import PartitionSpec as P

HEAD_DIM = 64
VALUE_DIM = 128
GROUP_DIM = 128
rope_base = 500000.0
head_scale = 0.8
norm_floor = 1e-06
head_floor = 0.001
masked_score = -1e30
pool_reach = 15
key_block = 1024


def from_behind(x, axis, by):
    peers = lax.axis_size(axis)
    pairs = [(i, i + by) for i in range(peers) if 0 <= i + by < peers]
    return lax.ppermute(x, axis, pairs)


def rotate(values_in, positions):
    half_dim = values_in.shape[-1] // 2
    inverse = rope_base ** (-(jnp.arange(half_dim, dtype=jnp.float32) * 2.0 / values_in.shape[-1]))
    angles = positions.astype(jnp.float32)[:, None] * inverse[None, :]
    cosine = jnp.cos(angles)[:, None, :]
    sine_part = jnp.sin(angles)[:, None, :]
    first_half = values_in[..., :half_dim]
    second_half = values_in[..., half_dim:]
    return jnp.concatenate(
        [
            first_half * cosine - second_half * sine_part,
            second_half * cosine + first_half * sine_part,
        ],
        axis=-1,
    )


def body(
    tokens,
    norm_gain,
    query_one,
    key_one,
    query_two,
    key_two,
    value_weight,
    pool_weight,
    lambda_head,
    head_gain,
    group_weight,
    pool_scale,
    out_attn,
    out_pool,
):
    tok_rows = tokens.shape[0]
    local_heads = query_one.shape[1] // HEAD_DIM
    local_groups = pool_weight.shape[1] // GROUP_DIM
    tp_index = lax.axis_index("tp")
    positions = lax.axis_index("sp") * tok_rows + jnp.arange(tok_rows, dtype=jnp.int32)
    score_scale = HEAD_DIM ** (-0.5)
    gathered = lax.all_gather(tokens, "tp", axis=1, tiled=True)
    float_rows = gathered.astype(jnp.float32)
    normed = (
        float_rows
        * lax.rsqrt(jnp.mean(float_rows * float_rows, axis=-1, keepdims=True) + norm_floor)
        * norm_gain
    ).astype(jnp.bfloat16)

    def contract(shard_part):
        return jnp.dot(normed, shard_part, preferred_element_type=jnp.float32)

    pieces = (
        lax.all_gather(query_one, "sp", axis=0, tiled=True),
        lax.all_gather(key_one, "sp", axis=0, tiled=True),
        lax.all_gather(query_two, "sp", axis=0, tiled=True),
        lax.all_gather(key_two, "sp", axis=0, tiled=True),
        lax.all_gather(value_weight, "sp", axis=0, tiled=True),
    )
    projected = tuple((contract(shard_part) for shard_part in pieces))
    pool_proj = contract(lax.all_gather(pool_weight, "sp", axis=0, tiled=True))

    def turned(flat_part):
        return rotate(flat_part.reshape(tok_rows, local_heads, HEAD_DIM), positions).astype(
            jnp.bfloat16
        )

    query_a = turned(projected[0])
    key_a = turned(projected[1]).reshape(tok_rows, local_heads * HEAD_DIM)
    query_b = turned(projected[2])
    key_b = turned(projected[3]).reshape(tok_rows, local_heads * HEAD_DIM)
    value_rows = projected[4].astype(jnp.bfloat16)
    queries = (query_a, query_b)
    initial = (
        jnp.full((2, tok_rows, local_heads), masked_score, jnp.float32),
        jnp.zeros((2, tok_rows, local_heads), jnp.float32),
        jnp.zeros((2, tok_rows, local_heads, VALUE_DIM), jnp.float32),
    )
    pieces = (
        lax.all_gather(key_a, "sp", axis=0, tiled=True),
        lax.all_gather(key_b, "sp", axis=0, tiled=True),
        lax.all_gather(value_rows, "sp", axis=0, tiled=True),
    )
    key_rows = pieces[0].shape[0]
    key_span = math.gcd(key_rows, key_block)
    count_blocks = key_rows // key_span
    stacked = tuple((member.reshape(count_blocks, key_span, local_heads, -1) for member in pieces))

    def step_block(carried, inputs):
        maxima, totals, accums = carried
        block_a, block_b, block_v, block_id = inputs
        key_pos = block_id * key_span + jnp.arange(key_span, dtype=jnp.int32)
        visible = (key_pos[None, :] <= positions[:, None])[:, None, :]
        new_maxima, new_totals, new_accums = ([], [], [])
        for map_index, key_part in enumerate((block_a, block_b)):
            scores = (
                jnp.einsum(
                    "qhd,khd->qhk", queries[map_index], key_part, preferred_element_type=jnp.float32
                )
                * score_scale
            )
            scores = jnp.where(visible, scores, masked_score)
            top_now = jnp.maximum(maxima[map_index], jnp.max(scores, axis=-1))
            factor = jnp.exp(maxima[map_index] - top_now)
            weights = jnp.where(visible, jnp.exp(scores - top_now[..., None]), 0.0)
            new_maxima.append(top_now)
            new_totals.append(totals[map_index] * factor + jnp.sum(weights, axis=-1))
            product = jnp.einsum(
                "qhk,khd->qhd",
                weights.astype(jnp.bfloat16),
                block_v,
                preferred_element_type=jnp.float32,
            )
            new_accums.append(accums[map_index] * factor[..., None] + product)
        return ((jnp.stack(new_maxima), jnp.stack(new_totals), jnp.stack(new_accums)), None)

    result_state, _ = lax.scan(
        step_block,
        initial,
        (stacked[0], stacked[1], stacked[2], jnp.arange(count_blocks, dtype=jnp.int32)),
    )
    maxima, totals, accums = result_state
    map_means = accums / totals[..., None]
    lambda_local = lax.dynamic_slice_in_dim(lambda_head, tp_index * local_heads, local_heads, 0)
    differed = map_means[0] - lambda_local[None, :, None] * map_means[1]
    scaled = (
        differed
        * lax.rsqrt(jnp.mean(differed * differed, axis=-1, keepdims=True) + head_floor)
        * head_gain
        * head_scale
    )
    attn_out = scaled.reshape(tok_rows, local_heads * VALUE_DIM).astype(jnp.bfloat16)
    pool_rows = pool_proj.astype(jnp.bfloat16)
    prior_rows = from_behind(pool_rows[tok_rows - pool_reach :], "sp", 1)
    extended = jnp.concatenate([prior_rows, pool_rows], axis=0).astype(jnp.float32)
    group_ids = tp_index * local_groups + jnp.arange(local_groups, dtype=jnp.int32)
    windows = jnp.left_shift(2, group_ids % 4)
    channel_windows = (windows[:, None] + jnp.zeros((1, GROUP_DIM), jnp.int32)).reshape(-1)
    window_sum = jnp.zeros((tok_rows, local_groups * GROUP_DIM), jnp.float32)
    for lag_steps in range(pool_reach + 1):
        keep_mask = (lag_steps < channel_windows).astype(jnp.float32)
        window_sum = (
            window_sum
            + extended[pool_reach - lag_steps : pool_reach - lag_steps + tok_rows]
            * keep_mask[None, :]
        )
    counts = jnp.minimum(positions[:, None] + 1, channel_windows[None, :]).astype(jnp.float32)
    window_mean = window_sum / counts - pool_rows.astype(jnp.float32)
    local_mixing = lax.dynamic_slice_in_dim(group_weight, tp_index * local_groups, local_groups, 0)
    grouped = jnp.einsum(
        "tgc,gcd->tgd",
        window_mean.astype(jnp.bfloat16).reshape(tok_rows, local_groups, GROUP_DIM),
        local_mixing,
        preferred_element_type=jnp.float32,
    )
    scale_local = lax.dynamic_slice_in_dim(
        pool_scale, tp_index * local_groups * GROUP_DIM, local_groups * GROUP_DIM, 0
    )
    pooled = (grouped.reshape(tok_rows, local_groups * GROUP_DIM) * scale_local).astype(
        jnp.bfloat16
    )
    attn_cols, pool_cols = (
        lax.all_gather(out_attn, "sp", axis=1, tiled=True),
        lax.all_gather(out_pool, "sp", axis=1, tiled=True),
    )
    return lax.psum_scatter(
        (
            jnp.dot(attn_out, attn_cols, preferred_element_type=jnp.float32)
            + jnp.dot(pooled, pool_cols, preferred_element_type=jnp.float32)
        ).astype(jnp.bfloat16),
        "tp",
        scatter_dimension=0,
        tiled=True,
    )


def solution(mesh):
    in_specs = (
        P("sp", "tp"),
        P(),
        P("sp", "tp"),
        P("sp", "tp"),
        P("sp", "tp"),
        P("sp", "tp"),
        P("sp", "tp"),
        P("sp", "tp"),
        P(),
        P(),
        P(),
        P(),
        P("tp", "sp"),
        P("tp", "sp"),
    )
    out_specs = P(("sp", "tp"), None)
    return jax.shard_map(body, mesh=mesh, in_specs=in_specs, out_specs=out_specs, check_vma=False)
```

profile of v0, /device:TPU:0, one launch (start us, length us, event | category | flops | bytes accessed | tf_op | source)
XLA Modules:
  0.0 335.7 jit_solution(8059476277659263844)
XLA Ops:
  6.5 0.7 all-gather.7.cloned.1.call-update
  7.3 0.7 all-gather.9.cloned.1.call-update
  8.1 0.7 all-gather.15.cloned.1.call-update
  8.8 19.6 %all-gather.7.cloned.1.call-done = bf16[256,2048]{1,0:T(8,128)(2,1)} async-done(((bf16[256,512]{1,0:T(8,128)(2,1)}), bf16[256,2048]{1,0:T(8,128)(2,1)}) %all-gather.7.cloned.1.call-update) | async-done | bytes 1048592 | tf_op jit(solution)/shard_map/all_gather | solution.py:64
  28.4 1.5 fusion.41
  29.9 1.6 fusion.43
  31.5 39.3 %all-gather.9.cloned.1.call-done = bf16[2048,256]{1,0:T(8,128)(2,1)} async-done(((bf16[256,256]{1,0:T(8,128)(2,1)}), bf16[2048,256]{1,0:T(8,128)(2,1)}) %all-gather.9.cloned.1.call-update) | async-done | bytes 1048592 | tf_op jit(solution)/shard_map/all_gather | solution.py:80
  70.8 2.3 convolution_convert_fusion.1
  75.6 31.9 %all_gather.37 = bf16[2048,128]{1,0:T(8,128)(2,1)S(1)} all-gather(bf16[256,128]{1,0:T(8,128)(2,1)S(1)} %copy-done.4), channel_id=1, replica_groups=mesh['sp'=8,'tp'=4] {'sp'}, dimensions={0}, use_global_device_ids=true | all-gather | bytes 589824 | tf_op jit(solution)/shard_map/all_gather | solution.py:77
  107.5 32.2 %all_gather.39 = bf16[2048,128]{1,0:T(8,128)(2,1)S(1)} all-gather(bf16[256,128]{1,0:T(8,128)(2,1)S(1)} %copy-done.5), channel_id=1, replica_groups=mesh['sp'=8,'tp'=4] {'sp'}, dimensions={0}, use_global_device_ids=true | all-gather | bytes 589824 | tf_op jit(solution)/shard_map/all_gather | solution.py:76
  139.7 32.3 %all_gather.40 = bf16[2048,128]{1,0:T(8,128)(2,1)S(1)} all-gather(bf16[256,128]{1,0:T(8,128)(2,1)S(1)} %copy-done.6), channel_id=1, replica_groups=mesh['sp'=8,'tp'=4] {'sp'}, dimensions={0}, use_global_device_ids=true | all-gather | bytes 589824 | tf_op jit(solution)/shard_map/all_gather | solution.py:79
  172.0 31.9 %all_gather.42 = bf16[2048,128]{1,0:T(8,128)(2,1)S(1)} all-gather(bf16[256,128]{1,0:T(8,128)(2,1)S(1)} %copy-done.7), channel_id=1, replica_groups=mesh['sp'=8,'tp'=4] {'sp'}, dimensions={0}, use_global_device_ids=true | all-gather | bytes 589824 | tf_op jit(solution)/shard_map/all_gather | solution.py:78
  204.1 0.7 dynamic_slice.24
  204.9 0.8 dynamic_slice.26
  207.8 32.2 %all_gather.41 = bf16[2048,128]{0,1:T(8,128)(2,1)S(1)} all-gather(bf16[256,128]{0,1:T(8,128)(2,1)S(1)} %bitcast.251), channel_id=1, replica_groups=mesh['sp'=8,'tp'=4] {'sp'}, dimensions={0}, use_global_device_ids=true | all-gather | bytes 589824 | tf_op jit(solution)/shard_map/all_gather | solution.py:103
  240.0 31.2 %all_gather.38 = bf16[2048,128]{0,1:T(8,128)(2,1)S(1)} all-gather(bf16[256,128]{0,1:T(8,128)(2,1)S(1)} %bitcast.252), channel_id=1, replica_groups=mesh['sp'=8,'tp'=4] {'sp'}, dimensions={0}, use_global_device_ids=true | all-gather | bytes 589824 | tf_op jit(solution)/shard_map/all_gather | solution.py:102
  271.1 1.7 convolution_convert_fusion
  272.8 1.5 collective-permute-start
  274.7 0.9 copy.23
  276.2 0.7 fusion.70
  277.1 1.3 reshape.313
  278.5 18.7 %while.15 = (s32[]{:T(128)}, f32[2,256,2]{1,2,0:T(2,128)S(1)}, f32[2,256,2]{1,2,0:T(2,128)S(1)}, f32[2,256,2,128]{1,3,2,0:T(8,128)S(1)}, s32[2]{0:T(128)S(1)}, /...) while((s32[]{:T(128)}, f32[2,256,2]{1,2,0:T(2,128)S(1)}, ...), condition=%wide.region_6.7_spmd.clone, body=%wide.region_1.6_spmd.clone.sunk | while | flops 416947456 | bytes 34822424 | solution.py:139
  278.6 0.7 dynamic_slice.53
  280.1 1.8 fusion.141
  282.8 2.4 fusion.147
  285.2 1.0 fusion.143
  289.5 1.8 fusion.141
  292.1 2.4 fusion.147
  294.5 1.0 fusion.143
  297.6 1.7 fusion.101
  299.4 2.7 fusion.40
  302.1 26.7 %reduce-scatter.2.cloned.1.call-done = bf16[64,2048]{1,0:T(8,128)(2,1)} async-done(((bf16[256,2048]{1,0:T(8,128)(2,1)}), bf16[64,2048]{1,0:T(8,128)(2,1)}) %reduce-scatter.2.cloned.1.call-update) | async-done | bytes 262160 | tf_op jit(solution)/shard_map/reduce_scatter | solution.py:188
  (105 shorter events, 12.4 us)
Async XLA Ops:
  6.5 269.7 %copy-start = (bf16[8,128,128]{2,1,0:T(8,128)(2,1)S(1)}, bf16[8,128,128]{2,1,0:T(8,128)(2,1)}, u32[]{:S(2)}) copy-start(bf16[8,128,128]{2,1,0:T(8,128)(2,1)} %param.26) | copy-start | bytes 786436
  6.5 21.8 %all-gather.7.cloned.1.call-start = ((), (), s32[]{:S(2)}) async-start(), calls=%async_computation.1 | async-start | bytes 1310720 | tf_op jit(solution)/shard_map/all_gather | solution.py:64
  7.3 63.5 %all-gather.9.cloned.1.call-start = ((), (), s32[]{:S(2)}) async-start(), calls=%async_computation.2 | async-start | bytes 1179648 | tf_op jit(solution)/shard_map/all_gather | solution.py:80
  8.0 263.1 %all-gather.15.cloned.1.call-start = ((), (), s32[]{:S(2)}) async-start(), calls=%async_computation.5 | async-start | bytes 1179648 | tf_op jit(solution)/shard_map/all_gather | solution.py:83
  8.7 268.4 %all-gather.11.cloned.1.call-start = ((), (), s32[]{:S(2)}) async-start(), calls=%async_computation.3 | async-start | bytes 1179648 | tf_op jit(solution)/shard_map/all_gather | solution.py:104
  29.9 45.7 %copy-start.4 = (bf16[256,128]{1,0:T(8,128)(2,1)S(1)}, bf16[256,128]{1,0:T(8,128)(2,1)}, u32[]{:S(2)}) copy-start(bf16[256,128]{1,0:T(8,128)(2,1)} %param.19) | copy-start | bytes 196612
  31.5 76.1 %copy-start.5 = (bf16[256,128]{1,0:T(8,128)(2,1)S(1)}, bf16[256,128]{1,0:T(8,128)(2,1)}, u32[]{:S(2)}) copy-start(bf16[256,128]{1,0:T(8,128)(2,1)} %param.18) | copy-start | bytes 196612
  31.5 108.2 %copy-start.6 = (bf16[256,128]{1,0:T(8,128)(2,1)S(1)}, bf16[256,128]{1,0:T(8,128)(2,1)}, u32[]{:S(2)}) copy-start(bf16[256,128]{1,0:T(8,128)(2,1)} %param.21) | copy-start | bytes 196612
  31.5 140.5 %copy-start.7 = (bf16[256,128]{1,0:T(8,128)(2,1)S(1)}, bf16[256,128]{1,0:T(8,128)(2,1)}, u32[]{:S(2)}) copy-start(bf16[256,128]{1,0:T(8,128)(2,1)} %param.20) | copy-start | bytes 196612
  31.5 173.4 %copy-start.8 = (f32[128]{0:T(128)S(1)}, f32[128]{0:T(128)}, u32[]{:S(2)}) copy-start(f32[128]{0:T(128)} %param.25) | copy-start | bytes 1540
  73.1 224.5 %all-gather.13.cloned.1.call-start = ((), (), s32[]{:S(2)}) async-start(), calls=%async_computation.4 | async-start | bytes 1179648 | tf_op jit(solution)/shard_map/all_gather | solution.py:185
  73.7 225.6 %all-gather.17.cloned.1.call-start = ((), (), s32[]{:S(2)}) async-start(), calls=%async_computation.6 | async-start | bytes 1179648 | tf_op jit(solution)/shard_map/all_gather | solution.py:186
  74.3 254.5 %reduce-scatter.2.cloned.1.call-start = ((), (), s32[]{:S(2)}) async-start(), calls=%async_computation.7 | async-start | bytes 1310720 | tf_op jit(solution)/shard_map/reduce_scatter | solution.py:188
  272.8 3.3 collective-permute-start
  274.3 1.9 copy-start.10
  274.3 1.9 copy-start.11
  278.5 3.4 %copy-start.2 = (bf16[2,1024,2,64]{1,3,2,0:T(8,128)(2,1)}, bf16[2,1024,2,64]{1,3,2,0:T(8,128)(2,1)S(1)}, u32[]{:S(2)}) copy-start(bf16[2,1024,2,64]{1,3,2,0:T(8,128)(2,1)S(1)} %get-tuple-element.317) | copy-start | bytes 1572868 | tf_op jit(solution)/shard_map/while
  282.8 2.4 copy-start.1
  282.8 2.4 copy-start.9
  286.9 1.0 copy-start.3
  287.9 3.4 %copy-start.2 = (bf16[2,1024,2,64]{1,3,2,0:T(8,128)(2,1)}, bf16[2,1024,2,64]{1,3,2,0:T(8,128)(2,1)S(1)}, u32[]{:S(2)}) copy-start(bf16[2,1024,2,64]{1,3,2,0:T(8,128)(2,1)S(1)} %get-tuple-element.317) | copy-start | bytes 1572868 | tf_op jit(solution)/shard_map/while
  292.1 2.4 copy-start.1
  292.1 2.4 copy-start.9
  296.2 1.0 copy-start.3
Sparse Core Ops, SparseCore 0:
  8.9 19.4 all-gather.6
  30.5 40.2 all-gather.8
  72.9 41.6 all-gather.14
  116.6 41.4 all-gather.10
  160.0 42.5 all-gather.12
  204.4 40.6 all-gather.16
  302.2 26.5 reduce-scatter.1
where the time goes:
time: 336 us
  blocking collectives  192 us (57%)
  waiting for transfers between devices  88.8 us (26%)
  matrix products  22.8 us (7%)
  between operations  13.8 us (4%)
  local copies, waits for them, and re-layouts  9.14 us (3%)
  other arithmetic  6.18 us (2%)
    all_gather x1, waiting for transfers between devices, body(): lax.all_gather(value_weight, 'sp', axis=0, tiled=True)  39.3 us
    all_gather x1, blocking collectives, body(): lax.all_gather(key_two, 'sp', axis=0, tiled=True)  32.3 us
    all_gather x1, blocking collectives, body(): lax.all_gather(key_b, 'sp', axis=0, tiled=True)  32.2 us
    all_gather x1, blocking collectives, body(): lax.all_gather(query_one, 'sp', axis=0, tiled=True)  32.2 us
    all_gather x1, blocking collectives, body(): lax.all_gather(query_two, 'sp', axis=0, tiled=True)  31.9 us
    all_gather x1, blocking collectives, body(): lax.all_gather(key_one, 'sp', axis=0, tiled=True)  31.9 us
    all_gather x1, blocking collectives, body(): lax.all_gather(key_a, 'sp', axis=0, tiled=True)  31.2 us
    reduce_scatter x1, waiting for transfers between devices, body(): lax.psum_scatter((jnp.dot(attn_out, attn_cols, preferred_element_type=jnp...  26.7 us
  transfers between devices with their start and end apart: 8, of which 3 were waited for; matrix products, arithmetic and copies ran while one was open for 10% of the time, Pallas kernels for 0%

commit v1 on v0

--- a/solution.py
+++ b/solution.py
@@ -14,6 +14,16 @@
 masked_score = -1e30
 pool_reach = 15
 key_block = 1024
+
+
+def pass_along(block, axis, along):
+    n_dev = lax.axis_size(axis)
+    held, shards = (block, [block])
+    for _ in range(n_dev - 1):
+        held = lax.ppermute(held, axis, [(i, (i + 1) % n_dev) for i in range(n_dev)])
+        shards.insert(0, held)
+    line = jnp.concatenate(shards, axis=along)
+    return jnp.roll(line, (lax.axis_index(axis) + 1) * block.shape[along], axis=along)
 
 
 def from_behind(x, axis, by):
@@ -61,7 +71,7 @@
     tp_index = lax.axis_index("tp")
     positions = lax.axis_index("sp") * tok_rows + jnp.arange(tok_rows, dtype=jnp.int32)
     score_scale = HEAD_DIM ** (-0.5)
-    gathered = lax.all_gather(tokens, "tp", axis=1, tiled=True)
+    gathered = pass_along(tokens, "tp", 1)
     float_rows = gathered.astype(jnp.float32)
     normed = (
         float_rows

time: 336 us -> 316 us (0.940)
  waiting for transfers between devices: 88.8 us -> 69.9 us
    all_gather x1 -> x0, waiting for transfers between devices: 19.6 us -> none  [body(): gathered = lax.all_gather(tokens, 'tp', axis=1, tiled=True)]
    ppermute x0 -> x3, waiting for transfers between devices: none -> 17.7 us  [pass_along(): lax.ppermute(held, axis, [(i, (i + 1) % n_dev) for i in range(n_dev)])]
    all_gather x1, waiting for transfers between devices: 39.3 us -> 24.9 us  [body(): lax.all_gather(value_weight, 'sp', axis=0, tiled=True)]
  transfers between devices with their start and end apart: 8 -> 10, of which waited for: 3 -> 5; matrix products, arithmetic and copies ran while one was open for 10% -> 10% of each run, Pallas kernels for 0% -> 0%
where the time goes in v1:
time: 316 us; the launch traced here: 315 us
  blocking collectives  192 us (61%)
  waiting for transfers between devices  69.9 us (22%)
  matrix products  22.7 us (7%)
  between operations  13.9 us (4%)
  local copies, waits for them, and re-layouts  9.66 us (3%)
  other arithmetic  3.75 us (1%)
    all_gather x1, blocking collectives, body(): lax.all_gather(query_two, 'sp', axis=0, tiled=True)  32.3 us
    all_gather x1, blocking collectives, body(): lax.all_gather(key_b, 'sp', axis=0, tiled=True)  32 us
    all_gather x1, blocking collectives, body(): lax.all_gather(key_two, 'sp', axis=0, tiled=True)  32 us
    all_gather x1, blocking collectives, body(): lax.all_gather(query_one, 'sp', axis=0, tiled=True)  31.9 us
    all_gather x1, blocking collectives, body(): lax.all_gather(key_one, 'sp', axis=0, tiled=True)  31.9 us
    all_gather x1, blocking collectives, body(): lax.all_gather(key_a, 'sp', axis=0, tiled=True)  31.5 us
    reduce_scatter x1, waiting for transfers between devices, body(): lax.psum_scatter((jnp.dot(attn_out, attn_cols, preferred_element_type=jnp...  25.4 us
    all_gather x1, waiting for transfers between devices, body(): lax.all_gather(value_weight, 'sp', axis=0, tiled=True)  24.9 us
  transfers between devices with their start and end apart: 10, of which 5 were waited for; matrix products, arithmetic and copies ran while one was open for 10% of the time, Pallas kernels for 0%

profile of v1, /device:TPU:0, one launch (start us, length us, event | category | flops | bytes accessed | tf_op | source)
XLA Modules:
  0.0 315.5 jit_solution(10207614538005891785)
XLA Ops:
  6.5 0.7 all-gather.6.cloned.1.call-update
  7.9 6.2 %collective-permute-done = bf16[256,512]{1,0:T(8,128)(2,1)S(1)} collective-permute-done((bf16[256,512]{1,0:T(8,128)(2,1)}, bf16[256,512]{1,0:T(8,128)(2,1)S(1)}, u32[]{:S(2)}, u32[]{:S(2)}) %collective-permute-start) | collective-permute-done | bytes 262176 | tf_op jit(solution)/shard_map/ppermute | solution.py:23
  14.1 5.8 %collective-permute-done.1 = bf16[256,512]{1,0:T(8,128)(2,1)S(1)} collective-permute-done((bf16[256,512]{1,0:T(8,128)(2,1)S(1)}, bf16[256,512]{1,0:T(8,128)(2,1)S(1)}, u32[]{:S(2)}, u32[]{:S(2)}) %collective-permute-start.1) | collective-permute-done | bytes 262176 | tf_op jit(solution)/shard_map/ppermute | solution.py:23
  20.0 5.7 %collective-permute-done.2 = bf16[256,512]{1,0:T(8,128)(2,1)S(1)} collective-permute-done((bf16[256,512]{1,0:T(8,128)(2,1)S(1)}, bf16[256,512]{1,0:T(8,128)(2,1)S(1)}, u32[]{:S(2)}, u32[]{:S(2)}) %collective-permute-start.2) | collective-permute-done | bytes 262176 | tf_op jit(solution)/shard_map/ppermute | solution.py:23
  25.8 1.0 constant_dynamic-update-slice_fusion.4
  27.6 24.9 %all-gather.6.cloned.1.call-done = bf16[2048,256]{1,0:T(8,128)(2,1)} async-done(((bf16[256,256]{1,0:T(8,128)(2,1)}), bf16[2048,256]{1,0:T(8,128)(2,1)}) %all-gather.6.cloned.1.call-update) | async-done | bytes 1048592 | tf_op jit(solution)/shard_map/all_gather | solution.py:90
  52.5 2.3 convolution_convert_fusion.1
  57.4 31.9 %all_gather.33 = bf16[2048,128]{1,0:T(8,128)(2,1)S(1)} all-gather(bf16[256,128]{1,0:T(8,128)(2,1)S(1)} %copy-done.5), channel_id=1, replica_groups=mesh['sp'=8,'tp'=4] {'sp'}, dimensions={0}, use_global_device_ids=true | all-gather | bytes 589824 | tf_op jit(solution)/shard_map/all_gather | solution.py:87
  89.2 31.9 %all_gather.35 = bf16[2048,128]{1,0:T(8,128)(2,1)S(1)} all-gather(bf16[256,128]{1,0:T(8,128)(2,1)S(1)} %copy-done.6), channel_id=1, replica_groups=mesh['sp'=8,'tp'=4] {'sp'}, dimensions={0}, use_global_device_ids=true | all-gather | bytes 589824 | tf_op jit(solution)/shard_map/all_gather | solution.py:86
  121.2 32.0 %all_gather.36 = bf16[2048,128]{1,0:T(8,128)(2,1)S(1)} all-gather(bf16[256,128]{1,0:T(8,128)(2,1)S(1)} %copy-done.7), channel_id=1, replica_groups=mesh['sp'=8,'tp'=4] {'sp'}, dimensions={0}, use_global_device_ids=true | all-gather | bytes 589824 | tf_op jit(solution)/shard_map/all_gather | solution.py:89
  153.2 32.3 %all_gather.38 = bf16[2048,128]{1,0:T(8,128)(2,1)S(1)} all-gather(bf16[256,128]{1,0:T(8,128)(2,1)S(1)} %copy-done.8), channel_id=1, replica_groups=mesh['sp'=8,'tp'=4] {'sp'}, dimensions={0}, use_global_device_ids=true | all-gather | bytes 589824 | tf_op jit(solution)/shard_map/all_gather | solution.py:88
  185.5 0.8 dynamic_slice.31
  188.7 32.0 %all_gather.37 = bf16[2048,128]{0,1:T(8,128)(2,1)S(1)} all-gather(bf16[256,128]{0,1:T(8,128)(2,1)S(1)} %bitcast.251), channel_id=1, replica_groups=mesh['sp'=8,'tp'=4] {'sp'}, dimensions={0}, use_global_device_ids=true | all-gather | bytes 589824 | tf_op jit(solution)/shard_map/all_gather | solution.py:113
  220.8 31.5 %all_gather.34 = bf16[2048,128]{0,1:T(8,128)(2,1)S(1)} all-gather(bf16[256,128]{0,1:T(8,128)(2,1)S(1)} %bitcast.252), channel_id=1, replica_groups=mesh['sp'=8,'tp'=4] {'sp'}, dimensions={0}, use_global_device_ids=true | all-gather | bytes 589824 | tf_op jit(solution)/shard_map/all_gather | solution.py:112
  252.2 1.7 convolution_convert_fusion
  253.9 1.5 collective-permute-start.3
  255.8 0.9 copy.23
  257.3 0.7 fusion.70
  258.2 1.3 reshape.313
  259.6 18.7 %while.15 = (s32[]{:T(128)}, f32[2,256,2]{1,2,0:T(2,128)S(1)}, f32[2,256,2]{1,2,0:T(2,128)S(1)}, f32[2,256,2,128]{1,3,2,0:T(8,128)S(1)}, s32[2]{0:T(128)S(1)}, /...) while((s32[]{:T(128)}, f32[2,256,2]{1,2,0:T(2,128)S(1)}, ...), condition=%wide.region_6.7_spmd.clone, body=%wide.region_1.6_spmd.clone.sunk | while | flops 416947456 | bytes 34822424 | solution.py:149
  259.6 0.7 dynamic_slice.60
  261.2 1.9 fusion.141
  263.9 2.4 fusion.147
  266.3 1.0 fusion.143
  267.3 0.6 fusion.146
  269.0 0.7 dynamic_slice.60
  270.6 1.9 fusion.141
  273.2 2.4 fusion.147
  275.6 1.0 fusion.143
  278.7 1.7 fusion.101
  280.5 2.7 fusion.40
  283.2 25.4 %reduce-scatter.2.cloned.1.call-done = bf16[64,2048]{1,0:T(8,128)(2,1)} async-done(((bf16[256,2048]{1,0:T(8,128)(2,1)}), bf16[64,2048]{1,0:T(8,128)(2,1)}) %reduce-scatter.2.cloned.1.call-update) | async-done | bytes 262160 | tf_op jit(solution)/shard_map/reduce_scatter | solution.py:198
  (122 shorter events, 12.6 us)
Async XLA Ops:
  6.5 250.7 %copy-start = (bf16[8,128,128]{2,1,0:T(8,128)(2,1)S(1)}, bf16[8,128,128]{2,1,0:T(8,128)(2,1)}, u32[]{:S(2)}) copy-start(bf16[8,128,128]{2,1,0:T(8,128)(2,1)} %param.26) | copy-start | bytes 786436
  6.5 20.3 %copy-start.1 = (bf16[256,512]{1,0:T(8,128)(2,1)S(1)}, bf16[256,512]{1,0:T(8,128)(2,1)}, u32[]{:S(2)}) copy-start(bf16[256,512]{1,0:T(8,128)(2,1)} %param.16) | copy-start | bytes 786436
  6.5 46.0 %all-gather.6.cloned.1.call-start = ((), (), s32[]{:S(2)}) async-start(), calls=%async_computation.1 | async-start | bytes 1179648 | tf_op jit(solution)/shard_map/all_gather | solution.py:90
  7.3 245.0 %all-gather.12.cloned.1.call-start = ((), (), s32[]{:S(2)}) async-start(), calls=%async_computation.4 | async-start | bytes 1179648 | tf_op jit(solution)/shard_map/all_gather | solution.py:93
  7.3 6.8 %collective-permute-start = (bf16[256,512]{1,0:T(8,128)(2,1)}, bf16[256,512]{1,0:T(8,128)(2,1)S(1)}, u32[]{:S(2)}, u32[]{:S(2)}) collective-permute-start(bf16[256,512]{1,0:T(8,128)(2,1)} %param.16), channel_id=1, source_target_pairs={{0,1},{1,2},{2,3},{3,0},{4,5},{5,6},{6,7},{7,4},{8,9},{9,10},{10,1... | collective-permute-start | bytes 786440 | tf_op jit(solution)/shard_map/ppermute | solution.py:23
  14.1 5.8 %collective-permute-start.1 = (bf16[256,512]{1,0:T(8,128)(2,1)S(1)}, bf16[256,512]{1,0:T(8,128)(2,1)S(1)}, u32[]{:S(2)}, u32[]{:S(2)}) collective-permute-start(bf16[256,512]{1,0:T(8,128)(2,1)S(1)} %collective-permute-done), channel_id=1, source_target_pairs={{0,1},{1,2},{2,3},{3,0},{4,5},{5,6},{6,7},{7,4},{8,9},{9,10},{10,1... | collective-permute-start | bytes 786440 | tf_op jit(solution)/shard_map/ppermute | solution.py:23
  19.9 5.8 %collective-permute-start.2 = (bf16[256,512]{1,0:T(8,128)(2,1)S(1)}, bf16[256,512]{1,0:T(8,128)(2,1)S(1)}, u32[]{:S(2)}, u32[]{:S(2)}) collective-permute-start(bf16[256,512]{1,0:T(8,128)(2,1)S(1)} %collective-permute-done.1), channel_id=1, source_target_pairs={{0,1},{1,2},{2,3},{3,0},{4,5},{5,6},{6,7},{7,4},{8,9},{9,10},{10,1... | collective-permute-start | bytes 786440 | tf_op jit(solution)/shard_map/ppermute | solution.py:23
  19.9 238.3 %all-gather.8.cloned.1.call-start = ((), (), s32[]{:S(2)}) async-start(), calls=%async_computation.2 | async-start | bytes 1179648 | tf_op jit(solution)/shard_map/all_gather | solution.py:114
  25.7 1.5 copy-start.9
  27.2 30.2 %copy-start.5 = (bf16[256,128]{1,0:T(8,128)(2,1)S(1)}, bf16[256,128]{1,0:T(8,128)(2,1)}, u32[]{:S(2)}) copy-start(bf16[256,128]{1,0:T(8,128)(2,1)} %param.19) | copy-start | bytes 196612
  27.5 61.7 %copy-start.6 = (bf16[256,128]{1,0:T(8,128)(2,1)S(1)}, bf16[256,128]{1,0:T(8,128)(2,1)}, u32[]{:S(2)}) copy-start(bf16[256,128]{1,0:T(8,128)(2,1)} %param.18) | copy-start | bytes 196612
  27.5 93.6 %copy-start.7 = (bf16[256,128]{1,0:T(8,128)(2,1)S(1)}, bf16[256,128]{1,0:T(8,128)(2,1)}, u32[]{:S(2)}) copy-start(bf16[256,128]{1,0:T(8,128)(2,1)} %param.21) | copy-start | bytes 196612
  27.5 125.7 %copy-start.8 = (bf16[256,128]{1,0:T(8,128)(2,1)S(1)}, bf16[256,128]{1,0:T(8,128)(2,1)}, u32[]{:S(2)}) copy-start(bf16[256,128]{1,0:T(8,128)(2,1)} %param.20) | copy-start | bytes 196612
  27.6 158.9 %copy-start.11 = (f32[8]{0:T(128)S(1)}, f32[8]{0:T(128)}, u32[]{:S(2)}) copy-start(f32[8]{0:T(128)} %param.24) | copy-start | bytes 100
  27.6 159.0 %copy-start.10 = (f32[128]{0:T(128)S(1)}, f32[128]{0:T(128)}, u32[]{:S(2)}) copy-start(f32[128]{0:T(128)} %param.25) | copy-start | bytes 1540
  54.8 223.9 %all-gather.10.cloned.1.call-start = ((), (), s32[]{:S(2)}) async-start(), calls=%async_computation.3 | async-start | bytes 1179648 | tf_op jit(solution)/shard_map/all_gather | solution.py:195
  55.4 225.0 %all-gather.14.cloned.1.call-start = ((), (), s32[]{:S(2)}) async-start(), calls=%async_computation.5 | async-start | bytes 1179648 | tf_op jit(solution)/shard_map/all_gather | solution.py:196
  56.0 252.6 %reduce-scatter.2.cloned.1.call-start = ((), (), s32[]{:S(2)}) async-start(), calls=%async_computation.6 | async-start | bytes 1310720 | tf_op jit(solution)/shard_map/reduce_scatter | solution.py:198
  253.9 3.3 %collective-permute-start.3 = (bf16[15,256]{1,0:T(8,128)(2,1)S(1)}, bf16[15,256]{1,0:T(8,128)(2,1)S(1)}, u32[]{:S(2)}, u32[]{:S(2)}) collective-permute-start(bf16[15,256]{1,0:T(8,128)(2,1)S(1)} %slice.144), channel_id=1, source_target_pairs={{0,4},{4,8},{8,12},{12,16},{16,20},{20,24},{24,28},{1,5},{5,9},{9,... | collective-permute-start | bytes 23048 | tf_op jit(solution)/shard_map/ppermute | solution.py:32
  255.4 1.9 copy-start.13
  255.4 1.9 copy-start.14
  259.6 3.4 %copy-start.3 = (bf16[2,1024,2,64]{1,3,2,0:T(8,128)(2,1)}, bf16[2,1024,2,64]{1,3,2,0:T(8,128)(2,1)S(1)}, u32[]{:S(2)}) copy-start(bf16[2,1024,2,64]{1,3,2,0:T(8,128)(2,1)S(1)} %get-tuple-element.317) | copy-start | bytes 1572868 | tf_op jit(solution)/shard_map/while
  263.9 2.4 copy-start.2
  263.9 2.4 copy-start.12
  268.0 1.0 copy-start.4
  269.0 3.4 %copy-start.3 = (bf16[2,1024,2,64]{1,3,2,0:T(8,128)(2,1)}, bf16[2,1024,2,64]{1,3,2,0:T(8,128)(2,1)S(1)}, u32[]{:S(2)}) copy-start(bf16[2,1024,2,64]{1,3,2,0:T(8,128)(2,1)S(1)} %get-tuple-element.317) | copy-start | bytes 1572868 | tf_op jit(solution)/shard_map/while
  273.2 2.4 copy-start.2
  273.2 2.4 copy-start.12
  277.3 1.0 copy-start.4
Sparse Core Ops, SparseCore 0:
  9.5 42.9 all-gather.5
  54.6 41.8 all-gather.11
  98.7 41.9 all-gather.7
  142.5 41.8 all-gather.9
  186.3 40.4 all-gather.13
  283.3 25.2 reduce-scatter.1
